TPU v7x, 32 devices: a whole 2x2x4 slice. The times are simulated.
32 devices in a mesh: ep: 8 (over z, y), tp: 4 (over x, core).
Axes of the slice: x: 2, y: 2, z: 4, core: 2. Of those that a mesh axis runs over, the one named last changes fastest.
Arguments:
- tokens: bfloat16 [1024, 2048], P('ep'), may hold values from -6 to 6
- norm_gain: float32 [2048], replicated, may hold values from 0.1 to 1.9
- routes: int32 [1024, 2], P('ep'), may hold values from 0 to 7, all different within a row; in each aligned block of 128 rows (0 to 127, 128 to 255, ...) at most 48 rows name the same one
- group_prob: float32 [1024], P('ep'), may hold values from 0.2 to 1
- expert_logits: float32 [1024, 2], P('ep'), may hold values from -6 to 6
- gate_weight: bfloat16 [8, 2048, 384], P('ep', None, 'tp'), may hold values from -0.125 to 0.125
- up_weight: bfloat16 [8, 2048, 384], P('ep', None, 'tp'), may hold values from -0.125 to 0.125
- down_matrix: bfloat16 [8, 384, 2048], P('ep', 'tp'), may hold values from -0.3125 to 0.3125
Outputs:
- combined: bfloat16 [1024, 2048], P('ep', 'tp')
Inputs may be any that keep to these rules, and one draw needn't show every extreme that they name: `routes`: each row names 2 different experts. Among the 128 tokens of one index of ep at most 48 rows name one expert, and in every draw some expert is named by exactly 48 of them.
All inputs are finite; a program needn't handle non-finite values.
Results may differ from a plain program's by a relative error of at most 0.013.
Values may be sent and summed in bfloat16 or wider, within the bound.
A program may use at most 64 MiB of HBM per device.

v0:
```python
import jax
import jax.numpy as jnp
from jax import lax
from jax.sharding import PartitionSpec as P


def hidden_part(buffer, gate_weight, up_weight):
    local_count = gate_weight.shape[0]
    grouped = buffer.reshape(
        buffer.shape[0] // local_count, local_count, buffer.shape[1], buffer.shape[2]
    )
    gate_proj = jnp.einsum(
        "sknd,kdf->sknf", grouped, gate_weight, preferred_element_type=jnp.float32
    )
    up_proj = jnp.einsum("sknd,kdf->sknf", grouped, up_weight, preferred_element_type=jnp.float32)
    hidden_state = (jax.nn.silu(gate_proj) * up_proj).astype(jnp.bfloat16)
    return hidden_state.reshape(buffer.shape[0], buffer.shape[1], hidden_state.shape[3])


def down_blocks(hidden_full, down_cols, block_count):
    local_count = down_cols.shape[0]
    width = hidden_full.shape[2] // block_count
    grouped = hidden_full.reshape(
        hidden_full.shape[0] // local_count, local_count, hidden_full.shape[1], block_count, width
    )
    columns = down_cols.reshape(local_count, block_count, width, down_cols.shape[2])
    block_list = jnp.einsum(
        "sknrf,krfd->sknrd", grouped, columns, preferred_element_type=jnp.float32
    ).astype(jnp.bfloat16)
    summed = jnp.sum(block_list.astype(jnp.float32), 3).astype(jnp.bfloat16)
    return summed.reshape(hidden_full.shape[0], hidden_full.shape[1], down_cols.shape[2])


def body(tokens, norm_gain, routes, group_prob, expert_logits, gate_weight, up_weight, down_matrix):
    tok_rows, model_width = tokens.shape
    top_count = routes.shape[1]
    experts = gate_weight.shape[0] * lax.axis_size("ep")
    capacity = 3 * top_count * tok_rows // (2 * experts)
    block_count = lax.axis_size("tp")
    down_cols = lax.all_to_all(down_matrix, "tp", split_axis=2, concat_axis=1, tiled=True)
    values = tokens.astype(jnp.float32)
    normed = (
        values * lax.rsqrt(jnp.mean(values * values, -1, keepdims=True) + 1e-06) * norm_gain
    ).astype(jnp.bfloat16)
    flat_ids = routes.reshape(-1)
    onehot = (flat_ids[:, None] == jnp.arange(experts, dtype=jnp.int32)[None, :]).astype(jnp.int32)
    earlier = jnp.cumsum(onehot, 0) - onehot
    slot_index = jnp.sum(earlier * onehot, 1)
    target = flat_ids * capacity + slot_index
    owners = jnp.arange(tok_rows * top_count, dtype=jnp.int32) // top_count
    outgoing = (
        jnp.zeros((experts * capacity, model_width), jnp.bfloat16).at[target].set(normed[owners])
    )
    outgoing = outgoing.reshape(experts, capacity, model_width)
    hidden_state = hidden_part(
        lax.all_to_all(outgoing, "ep", split_axis=0, concat_axis=0, tiled=True),
        gate_weight,
        up_weight,
    )
    hidden_full = lax.all_gather(hidden_state, "tp", axis=2, tiled=True)
    summed = down_blocks(hidden_full, down_cols, block_count)
    returned = lax.all_to_all(summed, "ep", split_axis=0, concat_axis=0, tiled=True)
    flat_back = returned.reshape(experts * capacity, returned.shape[2])
    weights = group_prob[:, None] * jax.nn.softmax(expert_logits, axis=-1)
    picked = flat_back[target].reshape(tok_rows, top_count, flat_back.shape[1]).astype(jnp.float32)
    combined = jnp.sum(picked * weights[:, :, None], 1).astype(jnp.bfloat16)
    return combined


def solution(mesh):
    return jax.shard_map(
        body,
        mesh=mesh,
        in_specs=(
            P("ep", None),
            P(),
            P("ep", None),
            P("ep"),
            P("ep", None),
            P("ep", None, "tp"),
            P("ep", None, "tp"),
            P("ep", "tp", None),
        ),
        out_specs=P("ep", "tp"),
        check_vma=False,
    )
```

profile of v0, /device:TPU:0, one launch (start us, length us, event | category | flops | bytes accessed | tf_op | source)
XLA Modules:
  0.0 104.3 jit_solution(11414660805682031129)
XLA Ops:
  0.0 2.4 %copy.32 = bf16[1,96,2048]{1,0,2:T(2,128)(2,1)S(1)} copy(bf16[1,96,2048]{2,1,0:T(8,128)(2,1)} %param.15) | data formatting | bytes 786432 | tf_op args[7]
  2.4 0.5 broadcast.137
  2.9 11.6 %reduce.6 = bf16[2048,96]{1,0:T(8,128)(2,1)S(1)} reduce(bf16[2048,1,96]{2,1,0:T(2,128)(2,1)S(1)} %bitcast.53, bf16[]{:T(256)} %broadcast.137), dimensions={1}, to_apply=%bitcast.44.reduce_sub_computation | reduce | bytes 786434
  14.5 1.6 %reshape.188 = bf16[4,2,24576]{2,1,0:T(2,128)(2,1)} reshape(bf16[2048,96]{1,0:T(8,128)(2,1)S(1)} %reduce.6) | data formatting | bytes 786432
  16.1 4.2 %all-to-all-start = ((bf16[4,2,24576]{2,1,0:T(2,128)(2,1)}), bf16[4,2,24576]{2,1,0:T(2,128)(2,1)S(1)}, u32[]{:S(2)}, u32[]{:S(2)}) async-start(bf16[4,2,24576]{2,1,0:T(2,128)(2,1)} %reshape.188), calls=%async_computation | async-start | bytes 786432 | tf_op jit(solution)/shard_map/all_to_all | solution.py:40
  20.7 0.6 reduce-window.6
  22.4 6.7 %scatter_custom_fusion = bf16[384,2048]{1,0:T(8,128)(2,1)} fusion(s32[256]{0:T(256)S(1)} %bitcast.57, bf16[128,2048]{1,0:T(8,128)(2,1)S(1)} %fusion.4, s32[1024]{0:T(1024)S(1)} %pad_clamp_fusion.1, bf16[]{:T(256)} %constant.32.clone.1), kind=kCustom, calls=%fused_computation.13 | custom fusion | bytes 1572866 | tf_op jit(solution)/shard_map/scatter | solution.py:52
  29.1 6.7 %all-to-all-start.1 = ((bf16[8,48,2048]{2,1,0:T(8,128)(2,1)}), bf16[8,48,2048]{2,1,0:T(8,128)(2,1)S(1)}, u32[]{:S(2)}, u32[]{:S(2)}) async-start(bf16[8,48,2048]{2,1,0:T(8,128)(2,1)} %bitcast.6), calls=%async_computation.1 | async-start | bytes 3145728 | tf_op jit(solution)/shard_map/all_to_all | solution.py:56
  35.9 0.8 reshape.189
  36.6 1.9 %fusion.14 = (bf16[1,96,512]{1,0,2:T(2,128)(2,1)}, bf16[1,96,512]{1,0,2:T(2,128)(2,1)S(1)}, bf16[1,96,512]{1,0,2:T(2,128)(2,1)S(1)}, bf16[1,96,512]{1,0,2:T(2,128)(2,1)}) fusion(bf16[1,96,2048]{1,0,2:T(2,128)(2,1)S(1)} %bitcast.52), kind=kLoop, calls=%fused_computation.40 | loop fusion | bytes 786432 | tf_op jit(solution)/shard_map/slice.2
  38.5 1.1 %copy.33 = bf16[1,96,512]{2,1,0:T(8,128)(2,1)S(1)} copy(bf16[1,96,512]{1,0,2:T(2,128)(2,1)} %get-tuple-element.5) | data formatting | bytes 196608 | tf_op jit(solution)/shard_map/slice.2
  39.6 1.1 %copy.34 = bf16[1,96,512]{2,1,0:T(8,128)(2,1)S(1)} copy(bf16[1,96,512]{1,0,2:T(2,128)(2,1)} %get-tuple-element.8) | data formatting | bytes 196608 | tf_op jit(solution)/shard_map/slice.3
  41.0 32.3 %all-to-all-done.1 = bf16[8,48,2048]{2,1,0:T(8,128)(2,1)S(1)} async-done(((bf16[8,48,2048]{2,1,0:T(8,128)(2,1)}), bf16[8,48,2048]{2,1,0:T(8,128)(2,1)S(1)}, u32[]{:S(2)}, u32[]{:S(2)}) %all-to-all-start.1) | async-done | bytes 1572896 | tf_op jit(solution)/shard_map/all_to_all | solution.py:56
  73.3 0.6 convolution_bitcast_fusion.1
  73.9 0.6 fusion.1
  74.6 8.7 %all-gather = bf16[8,1,48,384]{2,0,1,3:T(8,128)(2,1)S(1)} all-gather(bf16[8,1,48,96]{2,0,1,3:T(8,128)(2,1)S(1)} %copy.40), channel_id=2, replica_groups=mesh['ep'=8,'tp'=4] {'tp'}, dimensions={3}, use_global_device_ids=true | all-gather | bytes 368640 | tf_op jit(solution)/shard_map/all_gather | solution.py:60
  83.4 0.5 copy.42
  83.9 0.5 fusion.15
  84.4 1.1 %convert_reduce_fusion = bf16[512,8,48]{0,2,1:T(8,128)(2,1)} fusion(f32[4,512,8,48]{1,3,2,0:T(8,128)S(1)} %bitcast.51), kind=kLoop, calls=%fused_computation.3 | loop fusion | flops 1376256 | bytes 3538944 | tf_op jit(solution)/shard_map/reduce_sum | solution.py:30
  85.6 3.6 %all-to-all-start.2 = ((bf16[8,48,512]{2,1,0:T(8,128)(2,1)}), bf16[8,48,512]{2,1,0:T(8,128)(2,1)S(1)}, u32[]{:S(2)}, u32[]{:S(2)}) async-start(bf16[8,48,512]{2,1,0:T(8,128)(2,1)} %bitcast.23), calls=%async_computation.2 | async-start | bytes 786432 | tf_op jit(solution)/shard_map/all_to_all | solution.py:62
  89.4 12.0 %all-to-all-done.2 = bf16[8,48,512]{2,1,0:T(8,128)(2,1)S(1)} async-done(((bf16[8,48,512]{2,1,0:T(8,128)(2,1)}), bf16[8,48,512]{2,1,0:T(8,128)(2,1)S(1)}, u32[]{:S(2)}, u32[]{:S(2)}) %all-to-all-start.2) | async-done | bytes 393248 | tf_op jit(solution)/shard_map/all_to_all | solution.py:62
  101.4 1.2 %gather_fusion = bf16[256,512]{1,0:T(8,128)(2,1)S(1)} fusion(bf16[384,512]{1,0:T(8,128)(2,1)S(1)} %bitcast.50, s32[1024]{0:T(1024)S(1)} %pad_clamp_fusion), kind=kCustom, calls=%fused_computation.1 | custom fusion | bytes 525312 | tf_op jit(solution)/shard_map/gather | solution.py:65
  102.6 0.3 reshape.150
  102.9 1.4 %multiply_reduce_fusion = bf16[128,512]{1,0:T(8,128)(2,1)} fusion(f32[128,2,512]{2,1,0:T(2,128)S(1)} %reshape.150, f32[128,2]{1,0:T(8,128)S(1)} %copy.43), kind=kLoop, calls=%fused_computation.16 | loop fusion | flops 196608 | bytes 656384 | tf_op jit(solution)/shard_map/reduce_sum | solution.py:66
  (41 shorter events, 2.1 us)
Async XLA Ops:
  0.0 73.3 %copy-start = (bf16[1,2048,96]{1,2,0:T(8,128)(2,1)S(1)}, bf16[1,2048,96]{1,2,0:T(8,128)(2,1)}, u32[]{:S(2)}) copy-start(bf16[1,2048,96]{1,2,0:T(8,128)(2,1)} %param.13) | copy-start | bytes 1179652
  2.9 17.4 %copy-start.4 = (s32[128,2]{0,1:T(2,128)S(1)}, s32[128,2]{0,1:T(2,128)}, u32[]{:S(2)}) copy-start(s32[128,2]{0,1:T(2,128)} %param.10) | copy-start | bytes 3076
  2.9 19.0 %copy-start.1 = (bf16[128,2048]{1,0:T(8,128)(2,1)S(1)}, bf16[128,2048]{1,0:T(8,128)(2,1)}, u32[]{:S(2)}) copy-start(bf16[128,2048]{1,0:T(8,128)(2,1)} %param.8) | copy-start | bytes 1572868
  14.5 7.6 %copy-start.3 = (f32[2048]{0:T(1024)S(1)}, f32[2048]{0:T(1024)}, u32[]{:S(2)}) copy-start(f32[2048]{0:T(1024)} %param.9) | copy-start | bytes 24580
  16.1 13.1 %all-to-all-start = ((bf16[4,2,24576]{2,1,0:T(2,128)(2,1)}), bf16[4,2,24576]{2,1,0:T(2,128)(2,1)S(1)}, u32[]{:S(2)}, u32[]{:S(2)}) async-start(bf16[4,2,24576]{2,1,0:T(2,128)(2,1)} %reshape.188), calls=%async_computation | async-start | bytes 786432 | tf_op jit(solution)/shard_map/all_to_all | solution.py:40
  29.1 44.2 %all-to-all-start.1 = ((bf16[8,48,2048]{2,1,0:T(8,128)(2,1)}), bf16[8,48,2048]{2,1,0:T(8,128)(2,1)S(1)}, u32[]{:S(2)}, u32[]{:S(2)}) async-start(bf16[8,48,2048]{2,1,0:T(8,128)(2,1)} %bitcast.6), calls=%async_computation.1 | async-start | bytes 3145728 | tf_op jit(solution)/shard_map/all_to_all | solution.py:56
  40.9 33.0 %copy-start.6 = (bf16[1,2048,96]{1,2,0:T(8,128)(2,1)S(1)}, bf16[1,2048,96]{1,2,0:T(8,128)(2,1)}, u32[]{:S(2)}) copy-start(bf16[1,2048,96]{1,2,0:T(8,128)(2,1)} %param.14) | copy-start | bytes 1179652
  84.4 4.8 %copy-start.2 = (f32[128,2]{0,1:T(2,128)S(1)}, f32[128,2]{0,1:T(2,128)}, u32[]{:S(2)}) copy-start(f32[128,2]{0,1:T(2,128)} %param.12) | copy-start | bytes 3076
  84.4 4.8 %copy-start.5 = (f32[128]{0:T(128)S(1)}, f32[128]{0:T(128)}, u32[]{:S(2)}) copy-start(f32[128]{0:T(128)} %param.11) | copy-start | bytes 1540
  85.6 15.9 %all-to-all-start.2 = ((bf16[8,48,512]{2,1,0:T(8,128)(2,1)}), bf16[8,48,512]{2,1,0:T(8,128)(2,1)S(1)}, u32[]{:S(2)}, u32[]{:S(2)}) async-start(bf16[8,48,512]{2,1,0:T(8,128)(2,1)} %bitcast.23), calls=%async_computation.2 | async-start | bytes 786432 | tf_op jit(solution)/shard_map/all_to_all | solution.py:62
where the time goes:
time: 105 us; the launch traced here: 104 us
  waiting for transfers between devices  44.4 us (42%)
  local copies, waits for them, and re-layouts  19.4 us (18%)
  other arithmetic  15.3 us (15%)
  starting transfers between devices  14.6 us (14%)
  blocking collectives  8.74 us (8%)
  matrix products  1.68 us (2%)
    all_to_all x1, waiting for transfers between devices, body(): lax.all_to_all(outgoing, 'ep', split_axis=0, concat_axis=0, tiled=True)  32.3 us
    all_to_all x1, waiting for transfers between devices, body(): lax.all_to_all(summed, 'ep', split_axis=0, concat_axis=0, tiled=True)  12 us
    unnamed x1, other arithmetic  11.6 us
    all_gather x1, blocking collectives, body(): hidden_full = lax.all_gather(hidden_state, 'tp', axis=2, tiled=True)  8.74 us
    scatter x1, local copies, waits for them, and re-layouts, body(): jnp.zeros((experts * capacity, model_width), jnp.bfloat16).at[target]  6.74 us
    all_to_all x1, starting transfers between devices, body(): lax.all_to_all(outgoing, 'ep', split_axis=0, concat_axis=0, tiled=True)  6.73 us
    unnamed x19, local copies, waits for them, and re-layouts  5.36 us
    another operation x7, local copies, waits for them, and re-layouts  4.77 us
  transfers between devices with their start and end apart: 3, of which 2 were waited for; matrix products, arithmetic and copies ran while one was open for 13% of the time, Pallas kernels for 0%

commit v1 on v0

--- a/solution.py
+++ b/solution.py
@@ -57,7 +57,14 @@
         gate_weight,
         up_weight,
     )
-    hidden_full = lax.all_gather(hidden_state, "tp", axis=2, tiled=True)
+    peers = lax.axis_size("tp")
+    hops = [(i, (i + 1) % peers) for i in range(peers)]
+    parts = [hidden_state]
+    for stride in range(1, peers):
+        parts = [lax.ppermute(parts[0], "tp", hops), *parts]
+    whole = jnp.concatenate(parts, axis=2)
+    shift = (lax.axis_index("tp") + 1) * parts[-1].shape[2]
+    hidden_full = jnp.roll(whole, shift, axis=2)
     summed = down_blocks(hidden_full, down_cols, block_count)
     returned = lax.all_to_all(summed, "ep", split_axis=0, concat_axis=0, tiled=True)
     flat_back = returned.reshape(experts * capacity, returned.shape[2])

time: 105 us -> 96.3 us (0.917)
  blocking collectives: 8.74 us -> 0 us
  local copies, waits for them, and re-layouts: 19.4 us -> 16 us
  other arithmetic: 15.3 us -> 18 us
    all_to_all x1, waiting for transfers between devices: 32.3 us -> 22.6 us  [body(): lax.all_to_all(outgoing, 'ep', split_axis=0, concat_axis=0, tiled=True)]
    all_gather x1 -> x0, blocking collectives: 8.74 us -> none  [body(): hidden_full = lax.all_gather(hidden_state, 'tp', axis=2, tiled=True)]
    ppermute x0 -> x3, waiting for transfers between devices: none -> 6.44 us  [body(): parts = [lax.ppermute(parts[0], 'tp', hops), *parts]]
    all_to_all x1, waiting for transfers between devices: 0.01 us -> 6.27 us  [body(): lax.all_to_all(down_matrix, 'tp', split_axis=2, concat_axis=1, tiled=True)]
    another operation x7 -> x8, local copies, waits for them, and re-layouts: 4.77 us -> 1.88 us
    all_to_all x1, waiting for transfers between devices: 12 us -> 9.41 us  [body(): lax.all_to_all(summed, 'ep', split_axis=0, concat_axis=0, tiled=True)]
    unnamed x19 -> x15, local copies, waits for them, and re-layouts: 5.36 us -> 4.46 us
  transfers between devices with their start and end apart: 3 -> 6, of which waited for: 2 -> 5; matrix products, arithmetic and copies ran while one was open for 13% -> 19% of each run, Pallas kernels for 0% -> 0%
where the time goes in v1:
time: 96.3 us; the launch traced here: 95.8 us
  waiting for transfers between devices  44.7 us (46%)
  other arithmetic  18 us (19%)
  local copies, waits for them, and re-layouts  16 us (17%)
  starting transfers between devices  15.1 us (16%)
  matrix products  1.68 us (2%)
    all_to_all x1, waiting for transfers between devices, body(): lax.all_to_all(outgoing, 'ep', split_axis=0, concat_axis=0, tiled=True)  22.6 us
    unnamed x1, other arithmetic  11.5 us
    all_to_all x1, waiting for transfers between devices, body(): lax.all_to_all(summed, 'ep', split_axis=0, concat_axis=0, tiled=True)  9.41 us
    all_to_all x1, starting transfers between devices, body(): lax.all_to_all(outgoing, 'ep', split_axis=0, concat_axis=0, tiled=True)  7.44 us
    scatter x1, local copies, waits for them, and re-layouts, body(): jnp.zeros((experts * capacity, model_width), jnp.bfloat16).at[target]  6.74 us
    ppermute x3, waiting for transfers between devices, body(): parts = [lax.ppermute(parts[0], 'tp', hops), *parts]  6.44 us
    all_to_all x1, waiting for transfers between devices, body(): lax.all_to_all(down_matrix, 'tp', split_axis=2, concat_axis=1, tiled=True)  6.27 us
    unnamed x15, local copies, waits for them, and re-layouts  4.46 us
  transfers between devices with their start and end apart: 6, of which 5 were waited for; matrix products, arithmetic and copies ran while one was open for 19% of the time, Pallas kernels for 0%

profile of v1, /device:TPU:0, one launch (start us, length us, event | category | flops | bytes accessed | tf_op | source)
XLA Modules:
  0.0 95.8 jit_solution(1577492573152358375)
XLA Ops:
  0.0 0.8 copy.28
  1.1 0.7 broadcast_multiply_fusion
  1.8 0.6 reduce-window.6
  2.9 1.2 %fusion.3 = f32[128]{0:T(128)S(1)} fusion(bf16[128,2048]{1,0:T(8,128)(2,1)} %param.8), kind=kLoop, calls=%fused_computation.11 | loop fusion | flops 786304 | bytes 524800 | tf_op jit(solution)/shard_map/reduce_sum | solution.py:43
  4.3 1.2 %fusion.5 = bf16[128,2048]{1,0:T(8,128)(2,1)S(1)} fusion(bf16[128,2048]{1,0:T(8,128)(2,1)} %param.8, f32[2048]{0:T(1024)} %param.9, f32[128]{0:T(128)S(1)} %add_rsqrt_fusion), kind=kLoop, calls=%fused_computation.13 | loop fusion | flops 1048576 | bytes 1057280 | tf_op jit(solution)/shard_map/convert_element_type | solution.py:44
  5.5 6.7 %scatter_custom_fusion = bf16[384,2048]{1,0:T(8,128)(2,1)} fusion(s32[256]{0:T(256)S(1)} %bitcast.59, bf16[128,2048]{1,0:T(8,128)(2,1)S(1)} %fusion.5, s32[1024]{0:T(1024)S(1)} %pad_clamp_fusion.1, bf16[]{:T(256)} %constant.53.clone.1), kind=kCustom, calls=%fused_computation.14 | custom fusion | bytes 1572866 | tf_op jit(solution)/shard_map/scatter | solution.py:52
  12.3 7.4 %all-to-all-start.1 = ((bf16[8,48,2048]{2,1,0:T(8,128)(2,1)}), bf16[8,48,2048]{2,1,0:T(8,128)(2,1)S(1)}, u32[]{:S(2)}, u32[]{:S(2)}) async-start(bf16[8,48,2048]{2,1,0:T(8,128)(2,1)} %bitcast.6), calls=%async_computation.1 | async-start | bytes 3145728 | tf_op jit(solution)/shard_map/all_to_all | solution.py:56
  19.7 0.8 copy.22
  21.0 11.5 %reduce.6 = bf16[2048,96]{1,0:T(8,128)(2,1)S(1)} reduce(bf16[2048,1,96]{2,1,0:T(2,128)(2,1)S(1)} %bitcast.56, bf16[]{:T(256)} %broadcast.141), dimensions={1}, to_apply=%bitcast.47.reduce_sub_computation | reduce | bytes 786434
  32.5 1.6 %reshape.186 = bf16[4,2,24576]{2,1,0:T(2,128)(2,1)} reshape(bf16[2048,96]{1,0:T(8,128)(2,1)S(1)} %reduce.6) | data formatting | bytes 786432
  34.1 22.6 %all-to-all-done.1 = bf16[8,48,2048]{2,1,0:T(8,128)(2,1)S(1)} async-done(((bf16[8,48,2048]{2,1,0:T(8,128)(2,1)}), bf16[8,48,2048]{2,1,0:T(8,128)(2,1)S(1)}, u32[]{:S(2)}, u32[]{:S(2)}) %all-to-all-start.1) | async-done | bytes 1572896 | tf_op jit(solution)/shard_map/all_to_all | solution.py:56
  56.7 3.5 %all-to-all-start = ((bf16[4,2,24576]{2,1,0:T(2,128)(2,1)}), bf16[4,2,24576]{2,1,0:T(2,128)(2,1)S(1)}, u32[]{:S(2)}, u32[]{:S(2)}) async-start(bf16[4,2,24576]{2,1,0:T(2,128)(2,1)} %reshape.186), calls=%async_computation | async-start | bytes 786432 | tf_op jit(solution)/shard_map/all_to_all | solution.py:40
  60.2 0.6 convolution_bitcast_fusion.1
  60.8 0.6 fusion.2
  61.9 6.3 %all-to-all-done = bf16[4,2,24576]{2,1,0:T(2,128)(2,1)S(1)} async-done(((bf16[4,2,24576]{2,1,0:T(2,128)(2,1)}), bf16[4,2,24576]{2,1,0:T(2,128)(2,1)S(1)}, u32[]{:S(2)}, u32[]{:S(2)}) %all-to-all-start) | async-done | bytes 393248 | tf_op jit(solution)/shard_map/all_to_all | solution.py:40
  68.1 0.8 reshape.187
  69.0 1.1 %fusion.15 = (bf16[1,96,512]{1,0,2:T(2,128)(2,1)S(1)}, bf16[1,96,512]{1,0,2:T(2,128)(2,1)S(1)}, bf16[1,96,512]{1,0,2:T(2,128)(2,1)S(1)}, bf16[1,96,512]{1,0,2:T(2,128)(2,1)S(1)}) fusion(bf16[1,96,2048]{1,0,2:T(2,128)(2,1)S(1)} %bitcast.55), kind=kLoop, calls=%fused_computation.42 | loop fusion | bytes 786432 | tf_op jit(solution)/shard_map/slice.2
  70.6 2.4 %collective-permute-done.1 = bf16[8,48,96]{2,1,0:T(8,128)(2,1)S(1)} collective-permute-done((bf16[8,48,96]{2,1,0:T(8,128)(2,1)S(1)}, bf16[8,48,96]{2,1,0:T(8,128)(2,1)S(1)}, u32[]{:S(2)}, u32[]{:S(2)}) %collective-permute-start.1) | collective-permute-done | bytes 73760 | tf_op jit(solution)/shard_map/ppermute | solution.py:64
  73.0 4.0 %collective-permute-done.2 = bf16[8,48,96]{2,1,0:T(8,128)(2,1)S(1)} collective-permute-done((bf16[8,48,96]{2,1,0:T(8,128)(2,1)S(1)}, bf16[8,48,96]{2,1,0:T(8,128)(2,1)S(1)}, u32[]{:S(2)}, u32[]{:S(2)}) %collective-permute-start.2) | collective-permute-done | bytes 73760 | tf_op jit(solution)/shard_map/ppermute | solution.py:64
  78.6 1.1 %convert_reduce_fusion = bf16[512,8,48]{0,2,1:T(8,128)(2,1)} fusion(f32[4,512,8,48]{1,3,2,0:T(8,128)S(1)} %bitcast.54), kind=kLoop, calls=%fused_computation.3 | loop fusion | flops 1376256 | bytes 3538944 | tf_op jit(solution)/shard_map/reduce_sum | solution.py:30
  79.7 3.6 %all-to-all-start.2 = ((bf16[8,48,512]{2,1,0:T(8,128)(2,1)}), bf16[8,48,512]{2,1,0:T(8,128)(2,1)S(1)}, u32[]{:S(2)}, u32[]{:S(2)}) async-start(bf16[8,48,512]{2,1,0:T(8,128)(2,1)} %bitcast.23), calls=%async_computation.2 | async-start | bytes 786432 | tf_op jit(solution)/shard_map/all_to_all | solution.py:69
  83.6 9.4 %all-to-all-done.2 = bf16[8,48,512]{2,1,0:T(8,128)(2,1)S(1)} async-done(((bf16[8,48,512]{2,1,0:T(8,128)(2,1)}), bf16[8,48,512]{2,1,0:T(8,128)(2,1)S(1)}, u32[]{:S(2)}, u32[]{:S(2)}) %all-to-all-start.2) | async-done | bytes 393248 | tf_op jit(solution)/shard_map/all_to_all | solution.py:69
  93.0 1.2 %gather_fusion = bf16[256,512]{1,0:T(8,128)(2,1)S(1)} fusion(bf16[384,512]{1,0:T(8,128)(2,1)S(1)} %bitcast.53, s32[1024]{0:T(1024)S(1)} %pad_clamp_fusion), kind=kCustom, calls=%fused_computation.1 | custom fusion | bytes 525312 | tf_op jit(solution)/shard_map/gather | solution.py:72
  94.5 1.4 %multiply_reduce_fusion = bf16[128,512]{1,0:T(8,128)(2,1)} fusion(f32[128,2,512]{2,1,0:T(2,128)S(1)} %reshape.150, f32[128,2]{1,0:T(8,128)S(1)} %copy.31), kind=kLoop, calls=%fused_computation.17 | loop fusion | flops 196608 | bytes 656384 | tf_op jit(solution)/shard_map/reduce_sum | solution.py:73
  (44 shorter events, 4.5 us)
Async XLA Ops:
  0.0 60.2 %copy-start = (bf16[1,2048,96]{1,2,0:T(8,128)(2,1)S(1)}, bf16[1,2048,96]{1,2,0:T(8,128)(2,1)}, u32[]{:S(2)}) copy-start(bf16[1,2048,96]{1,2,0:T(8,128)(2,1)} %param.13) | copy-start | bytes 1179652
  12.3 7.4 %copy-start.1 = (bf16[1,96,2048]{2,1,0:T(8,128)(2,1)S(1)}, bf16[1,96,2048]{2,1,0:T(8,128)(2,1)}, u32[]{:S(2)}) copy-start(bf16[1,96,2048]{2,1,0:T(8,128)(2,1)} %param.15) | copy-start | bytes 1179652
  12.3 44.4 %all-to-all-start.1 = ((bf16[8,48,2048]{2,1,0:T(8,128)(2,1)}), bf16[8,48,2048]{2,1,0:T(8,128)(2,1)S(1)}, u32[]{:S(2)}, u32[]{:S(2)}) async-start(bf16[8,48,2048]{2,1,0:T(8,128)(2,1)} %bitcast.6), calls=%async_computation.1 | async-start | bytes 3145728 | tf_op jit(solution)/shard_map/all_to_all | solution.py:56
  34.1 26.7 %copy-start.4 = (bf16[1,2048,96]{1,2,0:T(8,128)(2,1)S(1)}, bf16[1,2048,96]{1,2,0:T(8,128)(2,1)}, u32[]{:S(2)}) copy-start(bf16[1,2048,96]{1,2,0:T(8,128)(2,1)} %param.14) | copy-start | bytes 1179652
  56.7 11.4 %all-to-all-start = ((bf16[4,2,24576]{2,1,0:T(2,128)(2,1)}), bf16[4,2,24576]{2,1,0:T(2,128)(2,1)S(1)}, u32[]{:S(2)}, u32[]{:S(2)}) async-start(bf16[4,2,24576]{2,1,0:T(2,128)(2,1)} %reshape.186), calls=%async_computation | async-start | bytes 786432 | tf_op jit(solution)/shard_map/all_to_all | solution.py:40
  61.3 7.6 %collective-permute-start = (bf16[8,48,96]{2,1,0:T(8,128)(2,1)S(1)}, bf16[8,48,96]{2,1,0:T(8,128)(2,1)S(1)}, u32[]{:S(2)}, u32[]{:S(2)}) collective-permute-start(bf16[8,48,96]{2,1,0:T(8,128)(2,1)S(1)} %fusion.2), channel_id=1, source_target_pairs={{0,1},{1,2},{2,3},{3,0},{4,5},{5,6},{6,7},{7,4},{8,9},{9,10},{10,1... | collective-permute-start | bytes 221192 | tf_op jit(solution)/shard_map/ppermute | solution.py:64
  68.9 4.1 %collective-permute-start.1 = (bf16[8,48,96]{2,1,0:T(8,128)(2,1)S(1)}, bf16[8,48,96]{2,1,0:T(8,128)(2,1)S(1)}, u32[]{:S(2)}, u32[]{:S(2)}) collective-permute-start(bf16[8,48,96]{2,1,0:T(8,128)(2,1)S(1)} %collective-permute-done), channel_id=1, source_target_pairs={{0,1},{1,2},{2,3},{3,0},{4,5},{5,6},{6,7},{7,4},{8,9},{9,10},{10,1... | collective-permute-start | bytes 221192 | tf_op jit(solution)/shard_map/ppermute | solution.py:64
  73.0 4.0 %collective-permute-start.2 = (bf16[8,48,96]{2,1,0:T(8,128)(2,1)S(1)}, bf16[8,48,96]{2,1,0:T(8,128)(2,1)S(1)}, u32[]{:S(2)}, u32[]{:S(2)}) collective-permute-start(bf16[8,48,96]{2,1,0:T(8,128)(2,1)S(1)} %collective-permute-done.1), channel_id=1, source_target_pairs={{0,1},{1,2},{2,3},{3,0},{4,5},{5,6},{6,7},{7,4},{8,9},{9,10},{10,1... | collective-permute-start | bytes 221192 | tf_op jit(solution)/shard_map/ppermute | solution.py:64
  78.6 4.8 %copy-start.2 = (f32[128,2]{0,1:T(2,128)S(1)}, f32[128,2]{0,1:T(2,128)}, u32[]{:S(2)}) copy-start(f32[128,2]{0,1:T(2,128)} %param.12) | copy-start | bytes 3076
  78.6 4.8 %copy-start.3 = (f32[128]{0:T(128)S(1)}, f32[128]{0:T(128)}, u32[]{:S(2)}) copy-start(f32[128]{0:T(128)} %param.11) | copy-start | bytes 1540
  79.7 13.2 %all-to-all-start.2 = ((bf16[8,48,512]{2,1,0:T(8,128)(2,1)}), bf16[8,48,512]{2,1,0:T(8,128)(2,1)S(1)}, u32[]{:S(2)}, u32[]{:S(2)}) async-start(bf16[8,48,512]{2,1,0:T(8,128)(2,1)} %bitcast.23), calls=%async_computation.2 | async-start | bytes 786432 | tf_op jit(solution)/shard_map/all_to_all | solution.py:69
